TPU v7x, 32 devices: a whole 2x2x4 slice. The times are simulated.
32 devices in a mesh: sp: 8 (over z, y), tp: 4 (over x, core).
Axes of the slice: x: 2, y: 2, z: 4, core: 2. Of those that a mesh axis runs over, the one named last changes fastest.
Arguments:
- query_rows: bfloat16 [4096, 2048], P('sp', 'tp'), may hold values from -40 to 40
- key_rows: bfloat16 [4096, 256], P('sp', 'tp'), may hold values from -6 to 6
- value_rows: bfloat16 [4096, 256], P('sp', 'tp'), may hold values from -12 to 12
- doc_ids: int32 [4096], P('sp'), may hold values from 0 to 3, never falling along the last dimension, each value on 1 to 2048 neighbouring positions
- sink_logit: float32 [32], P('tp'), may hold values from 1 to 6
- residual: bfloat16 [4096, 2048], P('sp'), may hold values from -10 to 10
- out_proj: bfloat16 [2048, 2048], P('tp'), may hold values from -0.25 to 0.25
- mix_gain: float32 [2048], replicated, may hold values from 0.1 to 1.9
- gate_proj: bfloat16 [2048, 5632], P('sp', 'tp'), may hold values from -0.125 to 0.125
- value_proj: bfloat16 [2048, 5632], P('sp', 'tp'), may hold values from -0.125 to 0.125
- gate_taps: float32 [3, 5632], P(None, 'tp'), may hold values from -3 to 3
- value_taps: float32 [3, 5632], P(None, 'tp'), may hold values from -3 to 3
- down_proj: bfloat16 [5632, 2048], P('tp', 'sp'), may hold values from -0.078125 to 0.078125
- final_gain: float32 [2048], P('tp'), may hold values from 0.1 to 1.9
Outputs:
- mixed: bfloat16 [4096, 2048], P('sp', 'tp')
All inputs are finite; a program needn't handle non-finite values.
Results may differ from a plain program's by a relative error of at most 0.012.
Values may be sent and summed in bfloat16 or wider, within the bound.
A program may use at most 128 MiB of HBM per device.

v0:
```python
import math

import jax
import jax.numpy as jnp
from jax import lax
from jax.sharding import PartitionSpec as P

HD = 64
WIN = 128
TAPS = 3


mix_scale = math.sqrt(2.0)
norm_eps = 1e-05


def passed_along(block, axis, distance):
    devices = range(lax.axis_size(axis))
    route = [(i - distance, i) for i in devices if i - distance in devices]
    return lax.ppermute(block, axis, route)


def attend(query_block, key_block, value_block, query_pos, key_pos, query_doc, key_doc, sink):
    head_size = query_block.shape[-1]
    scores = jnp.einsum(
        "qkgd,skd->kgqs", query_block, key_block, preferred_element_type=jnp.float32
    ) * head_size ** (-0.5)
    diff = query_pos[:, None] - key_pos[None, :]
    valid = (
        (diff >= 0)
        & (diff < WIN)
        & (query_doc[:, None] == key_doc[None, :])
        & (key_pos[None, :] >= 0)
    )
    scores = jnp.where(valid[None, None], scores, -1e30)
    top = jnp.maximum(jnp.max(scores, axis=-1, keepdims=True), sink)
    weights = jnp.exp(scores - top)
    total = jnp.sum(weights, axis=-1, keepdims=True) + jnp.exp(sink - top)
    probs = (weights / total).astype(jnp.bfloat16)
    out = jnp.einsum("kgqs,skd->qkgd", probs, value_block, preferred_element_type=jnp.float32)
    return out.astype(jnp.bfloat16)


def depthwise(tail, current, taps, tail_docs, docs):
    extended = jnp.concatenate([tail, current])
    ext_docs = jnp.concatenate([tail_docs, docs])
    lag_rows = tail.shape[0]
    count = current.shape[0]
    total = jnp.zeros(current.shape, jnp.float32)
    for lag in range(lag_rows + 1):
        start = lag_rows - lag
        same = (ext_docs[start : start + count] == docs)[:, None]
        rows = extended[start : start + count].astype(jnp.float32)
        total = total + taps[lag][None, :] * jnp.where(same, rows, 0.0)
    return total


def on_device(
    query_rows,
    key_rows,
    value_rows,
    doc_ids,
    sink_logit,
    residual,
    out_proj,
    mix_gain,
    gate_proj,
    value_proj,
    gate_taps,
    value_taps,
    down_proj,
    final_gain,
):
    rows = query_rows.shape[0]
    kv_local = key_rows.shape[1] // HD
    heads_local = query_rows.shape[1] // HD
    groups = heads_local // kv_local
    offset = lax.axis_index("sp") * rows
    prev_keys, prev_values, prev_docs = passed_along(
        (key_rows[rows - WIN :], value_rows[rows - WIN :], doc_ids[rows - WIN :]), "sp", 1
    )
    all_keys = jnp.concatenate([prev_keys, key_rows]).reshape(rows + WIN, kv_local, HD)
    all_values = jnp.concatenate([prev_values, value_rows]).reshape(rows + WIN, kv_local, HD)
    all_docs = jnp.concatenate([prev_docs, doc_ids])
    key_pos = offset - WIN + jnp.arange(rows + WIN, dtype=jnp.int32)
    query_pos = offset + jnp.arange(rows, dtype=jnp.int32)
    queries = query_rows.reshape(rows, kv_local, groups, HD)
    sink = sink_logit.reshape(kv_local, groups, 1, 1)
    pieces = attend(queries, all_keys, all_values, query_pos, key_pos, doc_ids, all_docs, sink)
    heads = pieces.reshape(rows, heads_local * HD)
    partial_value = jnp.dot(heads, out_proj, preferred_element_type=jnp.float32)
    width = residual.shape[1]
    share = width // lax.axis_size("tp")
    col_start = lax.axis_index("tp") * share
    attn_total = lax.psum(partial_value.astype(jnp.bfloat16), "tp").astype(jnp.float32)
    first_sum = mix_scale * residual.astype(jnp.float32) + attn_total
    mean = jnp.mean(first_sum, axis=1, keepdims=True)
    var = jnp.mean(jnp.square(first_sum - mean), axis=1, keepdims=True)
    normed = ((first_sum - mean) * lax.rsqrt(var + norm_eps) * mix_gain[None, :]).astype(
        jnp.bfloat16
    )
    normed_own = lax.dynamic_slice_in_dim(normed, col_start, share, 1)
    up_gate = jnp.dot(
        normed,
        lax.all_gather(gate_proj, "sp", axis=0, tiled=True),
        preferred_element_type=jnp.float32,
    )
    up_value = jnp.dot(
        normed,
        lax.all_gather(value_proj, "sp", axis=0, tiled=True),
        preferred_element_type=jnp.float32,
    )
    up_gate = up_gate.astype(jnp.bfloat16)
    up_value = up_value.astype(jnp.bfloat16)
    lag_rows = TAPS - 1
    prev_gate, prev_value = passed_along(
        (up_gate[rows - lag_rows :], up_value[rows - lag_rows :]), "sp", 1
    )
    tail_docs = prev_docs[WIN - lag_rows :]
    conv_gate = depthwise(prev_gate, up_gate, gate_taps, tail_docs, doc_ids)
    conv_value = depthwise(prev_value, up_value, value_taps, tail_docs, doc_ids)
    hidden = (jax.nn.gelu(conv_gate) * conv_value).astype(jnp.bfloat16)
    terms = jnp.dot(
        hidden,
        lax.all_gather(down_proj, "sp", axis=1, tiled=True),
        preferred_element_type=jnp.float32,
    )
    ffn_own = lax.psum_scatter(
        terms.astype(jnp.bfloat16), "tp", scatter_dimension=1, tiled=True
    ).astype(jnp.float32)
    second_sum = mix_scale * normed_own.astype(jnp.float32) + ffn_own
    row_sum, row_squares = lax.psum(
        (jnp.sum(second_sum, axis=1), jnp.sum(second_sum * second_sum, axis=1)), "tp"
    )
    mean = row_sum / width
    var = row_squares / width - mean * mean
    return (
        (second_sum - mean[:, None]) * lax.rsqrt(var + norm_eps)[:, None] * final_gain[None, :]
    ).astype(jnp.bfloat16)


def solution(mesh):
    placed = (
        P("sp", "tp"),
        P("sp", "tp"),
        P("sp", "tp"),
        P("sp"),
        P("tp"),
        P("sp", None),
        P("tp", None),
        P(),
        P("sp", "tp"),
        P("sp", "tp"),
        P(None, "tp"),
        P(None, "tp"),
        P("tp", "sp"),
        P("tp"),
    )
    return jax.shard_map(
        on_device, mesh=mesh, in_specs=placed, out_specs=P("sp", "tp"), check_vma=False
    )
```

profile of v0, /device:TPU:0, one launch (start us, length us, event | category | flops | bytes accessed | tf_op | source)
XLA Modules:
  0.0 373.8 jit_solution(1086754709857433635)
XLA Ops:
  8.2 4.9 %collective-permute-start.1 = (s32[128]{0:T(128)S(1)}, s32[128]{0:T(128)S(1)}, u32[]{:S(2)}, u32[]{:S(2)}) collective-permute-start(s32[128]{0:T(128)S(1)} %slice.57), channel_id=1, source_target_pairs={{0,4},{4,8},{8,12},{12,16},{16,20},{20,24},{24,28},{1,5},{5,9},{9,... | collective-permute-start | bytes 1544 | tf_op jit(solution)/shard_map/ppermute | solution.py:20
  13.8 3.4 collective-permute-start.2
  18.0 3.4 collective-permute-start
  21.4 1.3 copy.17
  23.4 1.4 fusion.21
  24.8 2.6 fusion.1
  27.5 2.1 fusion
  29.7 3.1 fusion.22
  32.9 2.6 convolution_convert_fusion.2
  37.7 48.6 %all-reduce.3.cloned.1.call-done = bf16[512,2048]{1,0:T(8,128)(2,1)} async-done(((bf16[512,2048]{1,0:T(8,128)(2,1)}), bf16[512,2048]{1,0:T(8,128)(2,1)}) %all-reduce.3.cloned.1.call-update) | async-done | bytes 2097168 | tf_op jit(solution)/shard_map/psum | solution.py:95
  86.3 3.1 fusion.4
  90.9 2.4 multiply_convert_fusion
  93.2 36.4 %all-gather.4.cloned.1.call-done = bf16[2048,1408]{1,0:T(8,128)(2,1)} async-done(((bf16[256,1408]{1,0:T(8,128)(2,1)}), bf16[2048,1408]{1,0:T(8,128)(2,1)}) %all-gather.4.cloned.1.call-update) | async-done | bytes 5767184 | tf_op jit(solution)/shard_map/all_gather | solution.py:105
  129.6 6.7 %convolution_convert_fusion.1 = bf16[512,1408]{1,0:T(8,128)(2,1)S(1)} fusion(bf16[512,2048]{1,0:T(8,128)(2,1)} %multiply_convert_fusion, bf16[2048,1408]{1,0:T(8,128)(2,1)} %all-gather.4.cloned.1.call-done), kind=kOutput, calls=%fused_computation.13 | convolution fusion | flops 2953510912 | bytes 9306112 | tf_op jit(solution)/shard_map/dot_general | solution.py:103
  137.5 2.5 collective-permute-start.3
  139.9 82.1 %all-gather.6.cloned.1.call-done = bf16[2048,1408]{1,0:T(8,128)(2,1)} async-done(((bf16[256,1408]{1,0:T(8,128)(2,1)}), bf16[2048,1408]{1,0:T(8,128)(2,1)}) %all-gather.6.cloned.1.call-update) | async-done | bytes 5767184 | tf_op jit(solution)/shard_map/all_gather | solution.py:110
  222.0 6.7 %convolution_convert_fusion = bf16[512,1408]{1,0:T(8,128)(2,1)S(1)} fusion(bf16[512,2048]{1,0:T(8,128)(2,1)} %multiply_convert_fusion, bf16[2048,1408]{1,0:T(8,128)(2,1)} %all-gather.6.cloned.1.call-done), kind=kOutput, calls=%fused_computation.12 | convolution fusion | flops 2953510912 | bytes 9306112 | tf_op jit(solution)/shard_map/dot_general | solution.py:108
  228.7 2.5 collective-permute-start.4
  231.3 83.8 %all-gather.8.cloned.1.call-done = bf16[1408,2048]{1,0:T(8,128)(2,1)} async-done(((bf16[1408,256]{1,0:T(8,128)(2,1)}), bf16[1408,2048]{1,0:T(8,128)(2,1)}) %all-gather.8.cloned.1.call-update) | async-done | bytes 5767184 | tf_op jit(solution)/shard_map/all_gather | solution.py:125
  315.1 12.0 %convolution_convert_fusion.3 = bf16[512,2048]{1,0:T(8,128)(2,1)} fusion(bf16[1408,2048]{1,0:T(8,128)(2,1)} %all-gather.8.cloned.1.call-done, bf16[512,1408]{1,0:T(8,128)(2,1)} %copy-done.11, bf16[512,1408]{1,0:T(8,128)(2,1)} %copy-done.10, bf16[2,1408]{1,0:T(2,128)(2,1)S(1)} %collective-permute-done.4, bf16[2,1408]{1,0:T(2,128)(2,1)S(1)} %collective-permute-done.3, ...), kind=kOutput, calls=%fused_computation.15 | convolution fusion | flops 2984116224 | bytes 10793984 | tf_op jit(solution)/shard_map/dot_general | solution.py:123
  327.1 29.5 %reduce-scatter.2.cloned.1.call-done = bf16[512,512]{1,0:T(8,128)(2,1)} async-done(((bf16[512,2048]{1,0:T(8,128)(2,1)}), bf16[512,512]{1,0:T(8,128)(2,1)}) %reduce-scatter.2.cloned.1.call-update) | async-done | bytes 524304 | tf_op jit(solution)/shard_map/reduce_scatter | solution.py:128
  356.6 1.5 fusion.25
  358.2 5.8 %all-reduce = (f32[512]{0:T(512)S(1)}, f32[512]{0:T(512)S(1)}) all-reduce(f32[512]{0:T(512)S(1)} %get-tuple-element.6, f32[512]{0:T(512)S(1)} %get-tuple-element.5), channel_id=1, replica_groups=mesh['sp'=8,'tp'=4] {'tp'}, use_global_device_ids=true, to_apply=%region_9.10 | all-reduce | flops 1024 | bytes 8192 | tf_op jit(solution)/shard_map/psum | solution.py:132
  363.9 2.3 multiply_convert_fusion.1
  (58 shorter events, 8.0 us)
Async XLA Ops:
  7.4 25.5 %copy-start = (bf16[512,2048]{1,0:T(8,128)(2,1)S(1)}, bf16[512,2048]{1,0:T(8,128)(2,1)}, u32[]{:S(2)}) copy-start(bf16[512,2048]{1,0:T(8,128)(2,1)} %param.20) | copy-start | bytes 6291460
  7.4 78.9 %all-reduce.3.cloned.1.call-start = ((), (), s32[]{:S(2)}) async-start(), calls=%async_computation.1 | async-start | bytes 4194304 | tf_op jit(solution)/shard_map/psum | solution.py:95
  8.2 14.5 %collective-permute-start.1 = (s32[128]{0:T(128)S(1)}, s32[128]{0:T(128)S(1)}, u32[]{:S(2)}, u32[]{:S(2)}) collective-permute-start(s32[128]{0:T(128)S(1)} %slice.57), channel_id=1, source_target_pairs={{0,4},{4,8},{8,12},{12,16},{16,20},{20,24},{24,28},{1,5},{5,9},{9,... | collective-permute-start | bytes 1544 | tf_op jit(solution)/shard_map/ppermute | solution.py:20
  13.8 11.0 %collective-permute-start.2 = (bf16[128,64]{0,1:T(8,128)(2,1)S(1)}, bf16[128,64]{0,1:T(8,128)(2,1)S(1)}, u32[]{:S(2)}, u32[]{:S(2)}) collective-permute-start(bf16[128,64]{0,1:T(8,128)(2,1)S(1)} %slice.58), channel_id=1, source_target_pairs={{0,4},{4,8},{8,12},{12,16},{16,20},{20,24},{24,28},{1,5},{5,9},{9,... | collective-permute-start | bytes 49160 | tf_op jit(solution)/shard_map/ppermute | solution.py:20
  18.0 11.7 %collective-permute-start = (bf16[128,64]{0,1:T(8,128)(2,1)S(1)}, bf16[128,64]{0,1:T(8,128)(2,1)S(1)}, u32[]{:S(2)}, u32[]{:S(2)}) collective-permute-start(bf16[128,64]{0,1:T(8,128)(2,1)S(1)} %slice.56), channel_id=1, source_target_pairs={{0,4},{4,8},{8,12},{12,16},{16,20},{20,24},{24,28},{1,5},{5,9},{9,... | collective-permute-start | bytes 49160 | tf_op jit(solution)/shard_map/ppermute | solution.py:20
  24.8 2.6 copy-start.9
  27.5 2.2 copy-start.7
  35.5 2.0 copy-start.4
  35.5 2.0 copy-start.5
  35.5 2.2 copy-start.3
  35.5 94.1 %all-gather.4.cloned.1.call-start = ((), (), s32[]{:S(2)}) async-start(), calls=%async_computation.2 | async-start | bytes 6488064 | tf_op jit(solution)/shard_map/all_gather | solution.py:105
  36.1 185.9 %all-gather.6.cloned.1.call-start = ((), (), s32[]{:S(2)}) async-start(), calls=%async_computation.3 | async-start | bytes 6488064 | tf_op jit(solution)/shard_map/all_gather | solution.py:110
  36.7 278.4 %all-gather.8.cloned.1.call-start = ((), (), s32[]{:S(2)}) async-start(), calls=%async_computation.4 | async-start | bytes 6488064 | tf_op jit(solution)/shard_map/all_gather | solution.py:125
  37.2 319.4 %reduce-scatter.2.cloned.1.call-start = ((), (), s32[]{:S(2)}) async-start(), calls=%async_computation.5 | async-start | bytes 2621440 | tf_op jit(solution)/shard_map/reduce_scatter | solution.py:128
  86.3 3.1 copy-start.1
  86.3 3.5 copy-start.2
  89.4 1.4 copy-start.6
  136.3 1.1 copy-start.10
  137.5 177.6 %collective-permute-start.3 = (bf16[2,1408]{1,0:T(2,128)(2,1)S(1)}, bf16[2,1408]{1,0:T(2,128)(2,1)S(1)}, u32[]{:S(2)}, u32[]{:S(2)}) collective-permute-start(bf16[2,1408]{1,0:T(2,128)(2,1)S(1)} %slice.74), channel_id=1, source_target_pairs={{0,4},{4,8},{8,12},{12,16},{16,20},{20,24},{24,28},{1,5},{5,9},{9,... | collective-permute-start | bytes 16904 | tf_op jit(solution)/shard_map/ppermute | solution.py:20
  228.7 2.5 copy-start.11
  228.7 86.3 %collective-permute-start.4 = (bf16[2,1408]{1,0:T(2,128)(2,1)S(1)}, bf16[2,1408]{1,0:T(2,128)(2,1)S(1)}, u32[]{:S(2)}, u32[]{:S(2)}) collective-permute-start(bf16[2,1408]{1,0:T(2,128)(2,1)S(1)} %slice.77), channel_id=1, source_target_pairs={{0,4},{4,8},{8,12},{12,16},{16,20},{20,24},{24,28},{1,5},{5,9},{9,... | collective-permute-start | bytes 16904 | tf_op jit(solution)/shard_map/ppermute | solution.py:20
  327.1 36.8 %copy-start.8 = (f32[512]{0:T(512)S(1)}, f32[512]{0:T(512)}, u32[]{:S(2)}) copy-start(f32[512]{0:T(512)} %param.27) | copy-start | bytes 6148
Sparse Core Ops, SparseCore 0:
  35.6 50.6 all-reduce.2
  327.2 29.3 reduce-scatter.1
Sparse Core Ops, SparseCore 1:
  38.2 91.4 all-gather.3
  131.7 90.3 all-gather.5
  223.9 91.1 all-gather.7
where the time goes:
time: 374 us
  waiting for transfers between devices  282 us (75%)
  matrix products  33.7 us (9%)
  starting transfers between devices  17 us (5%)
  between operations  15.3 us (4%)
  other arithmetic  14.9 us (4%)
  blocking collectives  5.76 us (2%)
  local copies, waits for them, and re-layouts  5.23 us (1%)
    all_gather x1, waiting for transfers between devices, on_device(): lax.all_gather(down_proj, 'sp', axis=1, tiled=True)  83.8 us
    all_gather x1, waiting for transfers between devices, on_device(): lax.all_gather(value_proj, 'sp', axis=0, tiled=True)  82.1 us
    psum x1, waiting for transfers between devices, on_device(): lax.psum(partial_value.astype(jnp.bfloat16), 'tp').astype(jnp.float32)  48.6 us
    all_gather x1, waiting for transfers between devices, on_device(): lax.all_gather(gate_proj, 'sp', axis=0, tiled=True)  36.4 us
    reduce_scatter x1, waiting for transfers between devices, on_device(): lax.psum_scatter(terms.astype(jnp.bfloat16), 'tp', scatter_dimension=1, t...  29.5 us
    ppermute x5, starting transfers between devices, passed_along(): return lax.ppermute(block, axis, route)  16.6 us
    dot_general x1, matrix products, on_device(): jnp.dot(hidden, lax.all_gather(down_proj, 'sp', axis=1, tiled=True), pref...  12 us
  transfers between devices with their start and end apart: 10, of which 5 were waited for; matrix products, arithmetic and copies ran while one was open for 8% of the time, Pallas kernels for 0%

commit v1 on v0

--- a/solution.py
+++ b/solution.py
@@ -1,8 +1,11 @@
+import functools
 import math
 
 import jax
 import jax.numpy as jnp
 from jax import lax
+from jax.experimental import pallas as pl
+from jax.experimental.pallas import tpu as pltpu
 from jax.sharding import PartitionSpec as P
 
 HD = 64
@@ -139,6 +142,565 @@
     ).astype(jnp.bfloat16)
 
 
+MESH = pl.DeviceIdType.MESH
+LANES = 128
+PAD = 16
+F32 = jnp.float32
+BF16 = jnp.bfloat16
+
+
+def ring_index(position, count):
+    position = lax.rem(position + 2 * count, count)
+    return jnp.where(position < count // 2, 2 * position, 2 * (count - 1 - position) + 1)
+
+
+def ring_position(index, count):
+    return jnp.where(lax.rem(index, 2) == 0, index // 2, count - 1 - index // 2)
+
+
+def layer_kernel(
+    n,
+    n_tp,
+    kv_ref,
+    docs_ref,
+    sink_ref,
+    query_ref,
+    out_proj_ref,
+    residual_ref,
+    mix_ref,
+    gate_ref,
+    value_ref,
+    gate_taps_ref,
+    value_taps_ref,
+    down_ref,
+    final_ref,
+    out_ref,
+    gate_all,
+    value_all,
+    down_all,
+    kv_ext,
+    docs_ext,
+    doc_cols,
+    queries,
+    proj,
+    rest,
+    heads,
+    parts,
+    parts_in,
+    normed,
+    up_gate,
+    up_value,
+    hidden,
+    terms,
+    terms_in,
+    second,
+    stats,
+    ring_send,
+    ring_recv,
+    local_sem,
+    halo_send,
+    halo_recv,
+    rows_send,
+    rows_recv,
+    norm_send,
+    norm_recv,
+    term_send,
+    term_recv,
+    stat_send,
+    stat_recv,
+):
+    sp = lax.axis_index("sp")
+    tp = lax.axis_index("tp")
+    rows = query_ref.shape[0]
+    ff = gate_ref.shape[1]
+    width = residual_ref.shape[1]
+    depth = gate_ref.shape[0]
+    cols = down_ref.shape[1]
+    share = width // n_tp
+    per = share // cols
+    steps = n // 2
+    here = ring_position(sp, n)
+    right = ring_index(here + 1, n)
+    left = ring_index(here - 1, n)
+    after = lax.rem(sp + 1, n)
+    before = lax.rem(sp + n - 1, n)
+    peers = [lax.rem(tp + i, n_tp) for i in range(1, n_tp)]
+
+    barrier = pltpu.get_barrier_semaphore()
+    for other in (right, left, after, before):
+        pl.semaphore_signal(barrier, inc=1, device_id=(other, tp), device_id_type=MESH)
+    for peer in peers:
+        pl.semaphore_signal(barrier, inc=1, device_id=(sp, peer), device_id_type=MESH)
+    pl.semaphore_wait(barrier, 4 + len(peers))
+
+    whole = (gate_all, value_all, down_all)
+    own = (gate_ref, value_ref, down_ref)
+    half_rows = (depth // 2, depth // 2, ff // 2)
+
+    def slot(w, index, half):
+        size = half_rows[w]
+        if w == 2:
+            return down_all.at[index, pl.ds(half * size, size)]
+        return whole[w].at[pl.ds(pl.multiple_of(index * depth + half * size, size), size)]
+
+    def sending(w, way, step, half):
+        if step == 1:
+            source = own[w].at[pl.ds(half * half_rows[w], half_rows[w])]
+            index = sp
+        else:
+            index = ring_index(here - (step - 1) if way == 0 else here + (step - 1), n)
+            source = slot(w, index, half)
+        return pltpu.make_async_remote_copy(
+            src_ref=source,
+            dst_ref=slot(w, index, half),
+            send_sem=ring_send.at[w, way, step - 1, half],
+            recv_sem=ring_recv.at[w, way, step - 1, half],
+            device_id=(right if way == 0 else left, tp),
+            device_id_type=MESH,
+        )
+
+    def arriving(w, way, step, half):
+        index = ring_index(here - step if way == 0 else here + step, n)
+        return pltpu.make_async_remote_copy(
+            src_ref=slot(w, index, half),
+            dst_ref=slot(w, index, half),
+            send_sem=ring_send.at[w, way, step - 1, half],
+            recv_sem=ring_recv.at[w, way, step - 1, half],
+            device_id=(right if way == 0 else left, tp),
+            device_id_type=MESH,
+        )
+
+    first_two = [
+        (w, step, half) for step in range(1, steps) for w in (0, 1) for half in (0, 1)
+    ] + [(0, steps, None), (1, steps, None)]
+    last = [(2, step, half) for step in range(1, steps) for half in (0, 1)] + [(2, steps, None)]
+    order = first_two + last
+    early = len(first_two)
+
+    def service(k):
+        w, step, half = order[k]
+        for way in (0, 1):
+            part = way if half is None else half
+            arriving(w, way, step, part).wait_recv()
+            if step < steps - 1 or (step == steps - 1 and part == way):
+                sending(w, way, step + 1, part).start()
+        if k in (early - 4, early - 3):
+            for way in (0, 1):
+                sending(2, way, 1, k - (early - 4)).start()
+
+    for w in (0, 1):
+        for half in (0, 1):
+            for way in (0, 1):
+                sending(w, way, 1, half).start()
+
+    halo = [
+        pltpu.make_async_remote_copy(
+            src_ref=kv_ref.at[pl.ds(rows - WIN, WIN)],
+            dst_ref=kv_ext.at[pl.ds(0, WIN)],
+            send_sem=halo_send.at[0],
+            recv_sem=halo_recv.at[0],
+            device_id=(after, tp),
+            device_id_type=MESH,
+        ),
+        pltpu.make_async_remote_copy(
+            src_ref=docs_ref.at[:, pl.ds(rows - WIN, WIN)],
+            dst_ref=docs_ext.at[:, pl.ds(0, WIN)],
+            send_sem=halo_send.at[1],
+            recv_sem=halo_recv.at[1],
+            device_id=(after, tp),
+            device_id_type=MESH,
+        ),
+    ]
+    for copy in halo:
+        copy.start()
+    row_share = rows // n_tp
+    fetch = [
+        pltpu.make_async_copy(kv_ref, kv_ext.at[pl.ds(WIN, rows)], local_sem.at[0]),
+        pltpu.make_async_copy(docs_ref, docs_ext.at[:, pl.ds(WIN, rows)], local_sem.at[1]),
+        pltpu.make_async_copy(query_ref, queries, local_sem.at[2]),
+        pltpu.make_async_copy(out_proj_ref, proj, local_sem.at[3]),
+        pltpu.make_async_copy(
+            residual_ref.at[pl.ds(pl.multiple_of(tp * row_share, row_share), row_share)],
+            rest,
+            local_sem.at[4],
+        ),
+        pltpu.make_async_copy(
+            gate_ref, gate_all.at[pl.ds(pl.multiple_of(sp * depth, depth), depth)], local_sem.at[5]
+        ),
+        pltpu.make_async_copy(
+            value_ref, value_all.at[pl.ds(pl.multiple_of(sp * depth, depth), depth)], local_sem.at[6]
+        ),
+        pltpu.make_async_copy(down_ref, down_all.at[sp], local_sem.at[7]),
+    ]
+    for copy in fetch:
+        copy.start()
+    for copy in fetch:
+        copy.wait()
+    for copy in halo:
+        copy.wait_recv()
+
+    line = lax.broadcasted_iota(jnp.int32, (LANES, LANES), 0)
+    lane = lax.broadcasted_iota(jnp.int32, (LANES, LANES), 1)
+    for b in range(rows // LANES + 1):
+        row = docs_ext[0:1, b * LANES : (b + 1) * LANES].astype(F32)
+        doc_cols[b * LANES : (b + 1) * LANES, :] = jnp.broadcast_to(row, (LANES, LANES)).T
+
+    low = lax.broadcasted_iota(jnp.int32, (2 * WIN, LANES), 1) < HD
+    zero = jnp.zeros((2 * WIN, LANES), BF16)
+
+    def attend_block(b, carry):
+        start = pl.multiple_of(b * WIN, WIN)
+        kv = kv_ext[pl.ds(start, 2 * WIN), 0:LANES]
+        vk = kv_ext[pl.ds(start, 2 * WIN), LANES : 2 * LANES]
+        keys = jnp.concatenate([jnp.where(low, kv, zero), jnp.where(low, zero, vk)], axis=0)
+        values = jnp.concatenate([jnp.where(low, vk, zero), jnp.where(low, zero, kv)], axis=0)
+        query_doc = doc_cols[pl.ds(start + WIN, WIN), :]
+        prev_doc = docs_ext[0:1, pl.ds(start, WIN)].astype(F32)
+        this_doc = docs_ext[0:1, pl.ds(start + WIN, WIN)].astype(F32)
+        prev_ok = (query_doc == prev_doc) & (lane > line) & (sp * rows + b * WIN > 0)
+        this_ok = (query_doc == this_doc) & (lane <= line)
+        bias = jnp.concatenate(
+            [jnp.where(prev_ok, 0.0, -1e30), jnp.where(this_ok, 0.0, -1e30)], axis=1
+        ).astype(F32)
+        for pair in range(query_ref.shape[1] // LANES):
+            block = queries[pl.ds(start, WIN), pair * LANES : (pair + 1) * LANES]
+            both = lax.dot_general(
+                block, keys, (((1,), (1,)), ((), ())), preferred_element_type=F32
+            )
+            probs = []
+            for side in (0, 1):
+                scores = both[:, side * 2 * WIN : (side + 1) * 2 * WIN] * HD ** (-0.5) + bias
+                sink = sink_ref[2 * pair + side]
+                top = jnp.maximum(jnp.max(scores, axis=1, keepdims=True), sink)
+                weights = jnp.exp(scores - top)
+                total = jnp.sum(weights, axis=1, keepdims=True) + jnp.exp(sink - top)
+                probs.append((weights / total).astype(BF16))
+            heads[:, pair * LANES : (pair + 1) * LANES] = jnp.dot(
+                jnp.concatenate(probs, axis=1), values, preferred_element_type=F32
+            ).astype(BF16)
+        for c in range(width // 512):
+            parts[b, :, c * 512 : (c + 1) * 512] = jnp.dot(
+                heads[...], proj[:, c * 512 : (c + 1) * 512], preferred_element_type=F32
+            ).astype(BF16)
+
+        for k in range(2):
+            @pl.when(b == k + 1)
+            def _():
+                service(k)
+
+        return carry
+
+    lax.fori_loop(0, n_tp, attend_block, 0)
+    done = 2
+
+    def rows_copy(peer, source):
+        return pltpu.make_async_remote_copy(
+            src_ref=parts.at[peer],
+            dst_ref=parts_in.at[source],
+            send_sem=rows_send.at[peer],
+            recv_sem=rows_recv.at[source],
+            device_id=(sp, peer),
+            device_id_type=MESH,
+        )
+
+    for peer in peers:
+        rows_copy(peer, tp).start()
+    for k in range(done, 5):
+        service(k)
+    done = 5
+    for peer in peers:
+        rows_copy(peer, peer).wait_recv()
+    at = pl.multiple_of(PAD + tp * row_share, PAD)
+    first = mix_scale * rest[...].astype(F32) + parts[tp].astype(F32)
+    for peer in peers:
+        first = first + parts_in[peer].astype(F32)
+    mean = jnp.mean(first, axis=1, keepdims=True)
+    first = first - mean
+    var = jnp.mean(first * first, axis=1, keepdims=True)
+    normed[pl.ds(at, row_share), :] = (first * lax.rsqrt(var + norm_eps) * mix_ref[...]).astype(
+        BF16
+    )
+
+    service(done)
+    done += 1
+
+    def norm_copy(peer, source):
+        place = pl.ds(pl.multiple_of(PAD + source * row_share, PAD), row_share)
+        return pltpu.make_async_remote_copy(
+            src_ref=normed.at[place],
+            dst_ref=normed.at[place],
+            send_sem=norm_send.at[peer],
+            recv_sem=norm_recv.at[source],
+            device_id=(sp, peer),
+            device_id_type=MESH,
+        )
+
+    for peer in peers:
+        norm_copy(peer, tp).start()
+    for k in range(done, 9):
+        service(k)
+    done = 9
+    for peer in peers:
+        norm_copy(peer, peer).wait_recv()
+    tail = pltpu.make_async_remote_copy(
+        src_ref=normed.at[pl.ds(rows, PAD)],
+        dst_ref=normed.at[pl.ds(0, PAD)],
+        send_sem=halo_send.at[2],
+        recv_sem=halo_recv.at[2],
+        device_id=(after, tp),
+        device_id_type=MESH,
+    )
+    tail.start()
+    for k in range(done, early):
+        service(k)
+    tail.wait_recv()
+
+    place = lax.broadcasted_iota(jnp.int32, (rows, LANES), 0) + sp * rows
+
+    def convolved(source, taps_ref, at):
+        total = taps_ref[0:1, pl.ds(at, LANES)] * source[PAD : PAD + rows, :]
+        doc = doc_cols[WIN : WIN + rows, :]
+        for lag in range(1, TAPS):
+            same = (doc_cols[WIN - lag : WIN - lag + rows, :] == doc) & (place >= lag)
+            shifted = jnp.where(same, source[PAD - lag : PAD - lag + rows, :], 0.0)
+            total = total + taps_ref[lag : lag + 1, pl.ds(at, LANES)] * shifted
+        return total
+
+    def up_block(c, carry):
+        at = pl.multiple_of(c * LANES, LANES)
+        weights = jnp.concatenate(
+            [gate_all[:, pl.ds(at, LANES)], value_all[:, pl.ds(at, LANES)]], axis=1
+        )
+        both = jnp.dot(normed[...], weights, preferred_element_type=F32)
+        both = both.astype(BF16).astype(F32)
+        up_gate[...] = both[:, :LANES]
+        up_value[...] = both[:, LANES:]
+        gate = convolved(up_gate, gate_taps_ref, at)
+        value = convolved(up_value, value_taps_ref, at)
+        inner = math.sqrt(2.0 / math.pi) * (gate + 0.044715 * (gate * gate * gate))
+        hidden[:, pl.ds(at, LANES)] = (0.5 * gate * (1.0 + jnp.tanh(inner)) * value).astype(BF16)
+        for k, when in ((0, 3), (1, 6), (2, 9)):
+            @pl.when(c == when)
+            def _():
+                service(early + k)
+
+        return carry
+
+    lax.fori_loop(0, ff // LANES, up_block, 0)
+
+    def term_copy(index, source):
+        owner = index // per
+        return pltpu.make_async_remote_copy(
+            src_ref=terms.at[index],
+            dst_ref=terms_in.at[source, lax.rem(index, per)],
+            send_sem=term_send.at[index],
+            recv_sem=term_recv.at[source, lax.rem(index, per)],
+            device_id=(sp, owner),
+            device_id_type=MESH,
+        )
+
+    def down_block(q, carry):
+        for k in range(3, len(last)):
+            @pl.when(q == 2 * (last[k][1] - 1) + 1)
+            def _():
+                service(early + k)
+
+        distance = (q + 1) // 2
+        index = ring_index(jnp.where(lax.rem(q, 2) == 1, here - distance, here + distance), n)
+        terms[index] = jnp.dot(
+            hidden[...], down_all[index], preferred_element_type=F32
+        ).astype(BF16)
+
+        @pl.when(index // per != tp)
+        def _():
+            term_copy(index, tp).start()
+
+        return carry
+
+    lax.fori_loop(0, n, down_block, 0)
+
+    for peer in peers:
+        for j in range(per):
+            pltpu.make_async_remote_copy(
+                src_ref=terms_in.at[peer, j],
+                dst_ref=terms_in.at[peer, j],
+                send_sem=term_send.at[0],
+                recv_sem=term_recv.at[peer, j],
+                device_id=(sp, peer),
+                device_id_type=MESH,
+            ).wait_recv()
+
+    sums = jnp.zeros((rows, 1), F32)
+    squares = jnp.zeros((rows, 1), F32)
+    for j in range(per):
+        mine = normed[PAD:, pl.ds(pl.multiple_of(tp * share + j * cols, cols), cols)]
+        total = mix_scale * mine.astype(F32) + terms[tp * per + j].astype(F32)
+        for peer in peers:
+            total = total + terms_in[peer, j].astype(F32)
+        second[:, j * cols : (j + 1) * cols] = total
+        sums = sums + jnp.sum(total, axis=1, keepdims=True)
+        squares = squares + jnp.sum(total * total, axis=1, keepdims=True)
+    which = lax.broadcasted_iota(jnp.int32, (rows, LANES), 1)
+    packed = jnp.where(which == 0, sums, jnp.where(which == 1, squares, 0.0))
+    stats[tp] = packed.T[0:8]
+
+    def stat_copy(peer, source):
+        return pltpu.make_async_remote_copy(
+            src_ref=stats.at[source],
+            dst_ref=stats.at[source],
+            send_sem=stat_send.at[peer],
+            recv_sem=stat_recv.at[source],
+            device_id=(sp, peer),
+            device_id_type=MESH,
+        )
+
+    for peer in peers:
+        stat_copy(peer, tp).start()
+    for peer in peers:
+        stat_copy(peer, peer).wait_recv()
+    total = stats[0]
+    for source in range(1, n_tp):
+        total = total + stats[source]
+    spread = jnp.concatenate([total] * (LANES // 8), axis=0).T
+    mean = spread[:, 0:1] / width
+    var = spread[:, 1:2] / width - mean * mean
+    out_ref[...] = (
+        (second[...] - mean) * lax.rsqrt(var + norm_eps) * final_ref[...]
+    ).astype(BF16)
+
+    for w in range(3):
+        for way in (0, 1):
+            for step in range(1, steps + 1):
+                for half in (0, 1):
+                    if step < steps or half == way:
+                        sending(w, way, step, half).wait_send()
+    for copy in halo:
+        copy.wait_send()
+    tail.wait_send()
+    for peer in peers:
+        rows_copy(peer, tp).wait_send()
+        norm_copy(peer, tp).wait_send()
+        stat_copy(peer, tp).wait_send()
+        for j in range(per):
+            term_copy(peer * per + j, tp).wait_send()
+
+
+def fused(
+    query_rows,
+    key_rows,
+    value_rows,
+    doc_ids,
+    sink_logit,
+    residual,
+    out_proj,
+    mix_gain,
+    gate_proj,
+    value_proj,
+    gate_taps,
+    value_taps,
+    down_proj,
+    final_gain,
+):
+    n = lax.axis_size("sp")
+    n_tp = lax.axis_size("tp")
+    rows, head_cols = query_rows.shape
+    width = residual.shape[1]
+    depth, ff = gate_proj.shape
+    cols = down_proj.shape[1]
+    per = width // n_tp // cols
+    steps = n // 2
+    kv = jnp.concatenate([key_rows, value_rows, value_rows, key_rows], axis=1)
+    docs = jnp.broadcast_to(doc_ids[None, :], (8, rows))
+    share = rows // n_tp
+    anywhere = pl.BlockSpec(memory_space=pl.ANY)
+    vmem = pl.BlockSpec(memory_space=pltpu.VMEM)
+    smem = pl.BlockSpec(memory_space=pltpu.SMEM)
+    dma = pltpu.SemaphoreType.DMA
+    return pl.pallas_call(
+        functools.partial(layer_kernel, n, n_tp),
+        out_shape=jax.ShapeDtypeStruct((rows, width // n_tp), BF16),
+        in_specs=[
+            anywhere, anywhere, smem, anywhere, anywhere, anywhere, vmem,
+            anywhere, anywhere, vmem, vmem, anywhere, vmem,
+        ],
+        out_specs=vmem,
+        scratch_shapes=[
+            pltpu.VMEM((n * depth, ff), BF16),
+            pltpu.VMEM((n * depth, ff), BF16),
+            pltpu.VMEM((n, ff, cols), BF16),
+            pltpu.VMEM((WIN + rows, 4 * HD), BF16),
+            pltpu.VMEM((8, WIN + rows), jnp.int32),
+            pltpu.VMEM((WIN + rows, LANES), F32),
+            pltpu.VMEM((rows, head_cols), BF16),
+            pltpu.VMEM((head_cols, width), BF16),
+            pltpu.VMEM((share, width), BF16),
+            pltpu.VMEM((share, head_cols), BF16),
+            pltpu.VMEM((n_tp, share, width), BF16),
+            pltpu.VMEM((n_tp, share, width), BF16),
+            pltpu.VMEM((PAD + rows, width), BF16),
+            pltpu.VMEM((PAD + rows, LANES), F32),
+            pltpu.VMEM((PAD + rows, LANES), F32),
+            pltpu.VMEM((rows, ff), BF16),
+            pltpu.VMEM((n, rows, cols), BF16),
+            pltpu.VMEM((n_tp, per, rows, cols), BF16),
+            pltpu.VMEM((rows, width // n_tp), F32),
+            pltpu.VMEM((n_tp, 8, rows), F32),
+            dma((3, 2, steps, 2)),
+            dma((3, 2, steps, 2)),
+            dma((8,)),
+            dma((3,)),
+            dma((3,)),
+            dma((n_tp,)),
+            dma((n_tp,)),
+            dma((n_tp,)),
+            dma((n_tp,)),
+            dma((n,)),
+            dma((n_tp, per)),
+            dma((n_tp,)),
+            dma((n_tp,)),
+        ],
+        compiler_params=pltpu.CompilerParams(
+            collective_id=0, has_side_effects=True, vmem_limit_bytes=60 * 1024 * 1024
+        ),
+        name="layer",
+    )(
+        kv,
+        docs,
+        sink_logit,
+        query_rows,
+        out_proj,
+        residual,
+        mix_gain[None, :],
+        gate_proj,
+        value_proj,
+        gate_taps,
+        value_taps,
+        down_proj,
+        final_gain[None, :],
+    )
+
+
+def on_any(*args):
+    query_rows, key_rows, gate_proj, down_proj = args[0], args[1], args[8], args[12]
+    n, n_tp = lax.axis_size("sp"), lax.axis_size("tp")
+    share = args[5].shape[1] // n_tp
+    depth, ff = gate_proj.shape
+    cols = down_proj.shape[1]
+    fits = (
+        n % 2 == 0
+        and n >= 8
+        and ff >= 10 * LANES
+        and query_rows.shape[0] == n_tp * WIN
+        and key_rows.shape[1] == HD
+        and query_rows.shape[1] % LANES == 0
+        and depth % 32 == 0
+        and ff % LANES == 0
+        and cols % LANES == 0
+        and share % cols == 0
+    )
+    return fused(*args) if fits else on_device(*args)
+
+
 def solution(mesh):
     placed = (
         P("sp", "tp"),
@@ -157,5 +719,5 @@
         P("tp"),
     )
     return jax.shard_map(
-        on_device, mesh=mesh, in_specs=placed, out_specs=P("sp", "tp"), check_vma=False
-    )
+        on_any, mesh=mesh, in_specs=placed, out_specs=P("sp", "tp"), check_vma=False
+    )

time: 374 us -> 201 us (0.54)
  waiting for transfers between devices: 282 us -> 0 us
  Pallas kernels: 0 us -> 194 us
  matrix products: 33.7 us -> 0 us
  starting transfers between devices: 17 us -> 0 us
  between operations: 15.3 us -> 0.02 us
  other arithmetic: 14.9 us -> 0.89 us
  blocking collectives: 5.76 us -> 0 us
    all_gather x3 -> x0, waiting for transfers between devices: 202 us -> none  [the longest x1 83.8 us: on_device(): lax.all_gather(down_proj, 'sp', axis=1, tiled=True)]
    pallas_call x0 -> x1, Pallas kernels: none -> 194 us  [fused(): pl.pallas_call(functools.partial(layer_kernel, n, n_tp), out_shape=jax.Sh...]
    psum x1 -> x0, waiting for transfers between devices: 48.6 us -> none  [on_device(): lax.psum(partial_value.astype(jnp.bfloat16), 'tp').astype(jnp.float32)]
    dot_general x6 -> x0, matrix products: 33.7 us -> none  [the longest x1 12 us: on_device(): jnp.dot(hidden, lax.all_gather(down_proj, 'sp', axis=1, tiled=True), pref...]
    reduce_scatter x1 -> x0, waiting for transfers between devices: 29.5 us -> none  [on_device(): lax.psum_scatter(terms.astype(jnp.bfloat16), 'tp', scatter_dimension=1, t...]
    ppermute x5 -> x0, starting transfers between devices: 16.6 us -> none  [passed_along(): return lax.ppermute(block, axis, route)]
    reduce_sum x4 -> x0, other arithmetic: 7.82 us -> none  [the longest x1 3.12 us: on_device(): mean = jnp.mean(first_sum, axis=1, keepdims=True)]
    psum x1 -> x0, blocking collectives: 5.76 us -> none  [on_device(): lax.psum((jnp.sum(second_sum, axis=1), jnp.sum(second_sum * second_sum, a...]
  transfers between devices with their start and end apart: 10 -> 0, of which waited for: 5 -> 0; matrix products, arithmetic and copies ran while one was open for 8% -> 0% of each run, Pallas kernels for 0% -> 0%
where the time goes in v1:
time: 201 us; the launch traced here: 200 us
  Pallas kernels  194 us (97%)
  local copies, waits for them, and re-layouts  5.06 us (3%)
    pallas_call x1, Pallas kernels, fused(): pl.pallas_call(functools.partial(layer_kernel, n, n_tp), out_shape=jax.Sh...  194 us

profile of v1, /device:TPU:0, one launch (start us, length us, event | category | flops | bytes accessed | tf_op | source)
XLA Modules:
  0.0 199.9 jit_solution(14985203950353346365)
XLA Ops:
  0.0 1.3 broadcast_in_dim.12.docs_ref
  1.3 1.0 copy.15
  2.2 1.0 copy.16
  3.2 0.9 pad_maximum_fusion.kv_ref
  4.1 193.9 %layer.1 = bf16[512,512]{1,0:T(8,128)(2,1)} custom-call(bf16[512,256]{1,0:T(8,128)(2,1)} %pad_maximum_fusion.kv_ref, s32[8,512]{1,0:T(8,128)} %broadcast_in_dim.12.docs_ref, f32[8]{0:T(128)} %sink_ref.1, bf16[512,512]{1,0:T(8,128)(2,1)} %query_ref.1, bf16[512,2048]{1,0:T(8,128)(2,1)} %out_proj_ref.1, bf16[512,2048]{1,0:T(8,128)(2,1)} %residual_ref.1, ...), custom_call_target="tpu_custom_call" | custom-call | tf_op jit(solution)/shard_map/layer/pallas_call | solution.py:619
  198.0 1.9 copy.20

commit v2 on v1

--- a/solution.py
+++ b/solution.py
@@ -149,15 +149,6 @@
 BF16 = jnp.bfloat16
 
 
-def ring_index(position, count):
-    position = lax.rem(position + 2 * count, count)
-    return jnp.where(position < count // 2, 2 * position, 2 * (count - 1 - position) + 1)
-
-
-def ring_position(index, count):
-    return jnp.where(lax.rem(index, 2) == 0, index // 2, count - 1 - index // 2)
-
-
 def layer_kernel(
     n,
     n_tp,
@@ -180,13 +171,19 @@
     down_all,
     kv_ext,
     docs_ext,
+    docs_other,
     doc_cols,
+    work_cols,
+    taps_gate,
+    taps_value,
     queries,
     proj,
     rest,
     heads,
     parts,
     parts_in,
+    norm_own,
+    norm_cols,
     normed,
     up_gate,
     up_value,
@@ -195,15 +192,23 @@
     terms_in,
     second,
     stats,
-    ring_send,
-    ring_recv,
+    plane_send,
+    row_send,
+    core_send,
+    block_recv,
     local_sem,
+    taps_send,
+    taps_recv,
     halo_send,
     halo_recv,
     rows_send,
     rows_recv,
     norm_send,
     norm_recv,
+    cols_send,
+    cols_recv,
+    tail_send,
+    tail_recv,
     term_send,
     term_recv,
     stat_send,
@@ -218,80 +223,105 @@
     cols = down_ref.shape[1]
     share = width // n_tp
     per = share // cols
-    steps = n // 2
-    here = ring_position(sp, n)
-    right = ring_index(here + 1, n)
-    left = ring_index(here - 1, n)
+    planes = n // 2
+    z, y = sp // 2, lax.rem(sp, 2)
+    x, core = tp // 2, lax.rem(tp, 2)
+    low = lax.rem(z, 2)
+    home = low == core
+    base = sp - 2 * low
+    work = base + 2 * core
+    unit = 2 * x + low
+    partner = base + 2 * (1 - low)
+    sibling = 2 * x + 1 - core
+    across = 2 * z + 1 - y
     after = lax.rem(sp + 1, n)
-    before = lax.rem(sp + n - 1, n)
     peers = [lax.rem(tp + i, n_tp) for i in range(1, n_tp)]
+    everyone = n * n_tp
+    me = sp * n_tp + tp
 
     barrier = pltpu.get_barrier_semaphore()
-    for other in (right, left, after, before):
-        pl.semaphore_signal(barrier, inc=1, device_id=(other, tp), device_id_type=MESH)
-    for peer in peers:
-        pl.semaphore_signal(barrier, inc=1, device_id=(sp, peer), device_id_type=MESH)
-    pl.semaphore_wait(barrier, 4 + len(peers))
+
+    def greet(i, carry):
+        other = lax.rem(me + i, everyone)
+        pl.semaphore_signal(
+            barrier,
+            inc=1,
+            device_id=(other // n_tp, lax.rem(other, n_tp)),
+            device_id_type=MESH,
+        )
+        return carry
+
+    lax.fori_loop(1, everyone, greet, 0)
+    pl.semaphore_wait(barrier, everyone - 1)
 
     whole = (gate_all, value_all, down_all)
     own = (gate_ref, value_ref, down_ref)
-    half_rows = (depth // 2, depth // 2, ff // 2)
-
-    def slot(w, index, half):
-        size = half_rows[w]
+
+    def slot(w, index):
         if w == 2:
-            return down_all.at[index, pl.ds(half * size, size)]
-        return whole[w].at[pl.ds(pl.multiple_of(index * depth + half * size, size), size)]
-
-    def sending(w, way, step, half):
-        if step == 1:
-            source = own[w].at[pl.ds(half * half_rows[w], half_rows[w])]
-            index = sp
-        else:
-            index = ring_index(here - (step - 1) if way == 0 else here + (step - 1), n)
-            source = slot(w, index, half)
+            return down_all.at[index]
+        return whole[w].at[pl.ds(pl.multiple_of(index * depth, depth), depth)]
+
+    def to_plane(w, i):
+        return pltpu.make_async_remote_copy(
+            src_ref=own[w],
+            dst_ref=slot(w, sp),
+            send_sem=plane_send.at[w, i],
+            recv_sem=block_recv.at[w, sp],
+            device_id=(2 * (core + 2 * i) + y, tp),
+            device_id_type=MESH,
+        )
+
+    def forward(w, index, source, sems, where, device):
         return pltpu.make_async_remote_copy(
             src_ref=source,
-            dst_ref=slot(w, index, half),
-            send_sem=ring_send.at[w, way, step - 1, half],
-            recv_sem=ring_recv.at[w, way, step - 1, half],
-            device_id=(right if way == 0 else left, tp),
-            device_id_type=MESH,
-        )
-
-    def arriving(w, way, step, half):
-        index = ring_index(here - step if way == 0 else here + step, n)
-        return pltpu.make_async_remote_copy(
-            src_ref=slot(w, index, half),
-            dst_ref=slot(w, index, half),
-            send_sem=ring_send.at[w, way, step - 1, half],
-            recv_sem=ring_recv.at[w, way, step - 1, half],
-            device_id=(right if way == 0 else left, tp),
-            device_id_type=MESH,
-        )
-
-    first_two = [
-        (w, step, half) for step in range(1, steps) for w in (0, 1) for half in (0, 1)
-    ] + [(0, steps, None), (1, steps, None)]
-    last = [(2, step, half) for step in range(1, steps) for half in (0, 1)] + [(2, steps, None)]
-    order = first_two + last
-    early = len(first_two)
-
-    def service(k):
-        w, step, half = order[k]
-        for way in (0, 1):
-            part = way if half is None else half
-            arriving(w, way, step, part).wait_recv()
-            if step < steps - 1 or (step == steps - 1 and part == way):
-                sending(w, way, step + 1, part).start()
-        if k in (early - 4, early - 3):
-            for way in (0, 1):
-                sending(2, way, 1, k - (early - 4)).start()
-
-    for w in (0, 1):
-        for half in (0, 1):
-            for way in (0, 1):
-                sending(w, way, 1, half).start()
+            dst_ref=slot(w, index),
+            send_sem=sems.at[w, where],
+            recv_sem=block_recv.at[w, index],
+            device_id=device,
+            device_id_type=MESH,
+        )
+
+    def to_row(w, at, source):
+        return forward(w, 2 * at + y, source, row_send, at, (across, tp))
+
+    def to_core(w, index, source):
+        return forward(w, index, source, core_send, index, (sp, sibling))
+
+    def await_block(w, index):
+        to_core(w, index, slot(w, index)).wait_recv()
+
+    def pass_own(w):
+        to_row(w, z, own[w]).start()
+        to_core(w, sp, own[w]).start()
+
+    def service(kind, w, j):
+        at = lax.rem(z + j, planes)
+
+        @pl.when(home)
+        def _():
+            if kind == "own":
+                pass_own(w)
+            elif kind == "col":
+                await_block(w, 2 * at + y)
+                to_row(w, at, slot(w, 2 * at + y)).start()
+                to_core(w, 2 * at + y, slot(w, 2 * at + y)).start()
+            else:
+                await_block(w, 2 * at + 1 - y)
+                to_core(w, 2 * at + 1 - y, slot(w, 2 * at + 1 - y)).start()
+
+    def plane_step(w):
+        for i in range(planes // 2):
+            @pl.when(core + 2 * i != z)
+            def _():
+                if w > 0:
+                    to_plane(w - 1, i).wait_send()
+                if w < 3:
+                    to_plane(w, i).start()
+
+    plane_step(0)
+    service("own", 0, 0)
+    service("own", 1, 0)
 
     halo = [
         pltpu.make_async_remote_copy(
@@ -324,20 +354,44 @@
             rest,
             local_sem.at[4],
         ),
-        pltpu.make_async_copy(
-            gate_ref, gate_all.at[pl.ds(pl.multiple_of(sp * depth, depth), depth)], local_sem.at[5]
-        ),
-        pltpu.make_async_copy(
-            value_ref, value_all.at[pl.ds(pl.multiple_of(sp * depth, depth), depth)], local_sem.at[6]
-        ),
-        pltpu.make_async_copy(down_ref, down_all.at[sp], local_sem.at[7]),
     ]
     for copy in fetch:
         copy.start()
+    settle = [pltpu.make_async_copy(own[w], slot(w, sp), local_sem.at[5 + w]) for w in range(3)]
+    settle.append(pltpu.make_async_copy(gate_taps_ref, taps_gate, local_sem.at[8]))
+    settle.append(pltpu.make_async_copy(value_taps_ref, taps_value, local_sem.at[9]))
+    taps = [
+        pltpu.make_async_remote_copy(
+            src_ref=source,
+            dst_ref=target,
+            send_sem=taps_send.at[i],
+            recv_sem=taps_recv.at[i],
+            device_id=(sp, sibling),
+            device_id_type=MESH,
+        )
+        for i, (source, target) in enumerate(
+            ((gate_taps_ref, taps_gate), (value_taps_ref, taps_value))
+        )
+    ]
+
+    @pl.when(home)
+    def _():
+        for copy in settle + taps:
+            copy.start()
+
     for copy in fetch:
         copy.wait()
     for copy in halo:
         copy.wait_recv()
+    docs_copy = pltpu.make_async_remote_copy(
+        src_ref=docs_ext,
+        dst_ref=docs_other,
+        send_sem=halo_send.at[2],
+        recv_sem=halo_recv.at[2],
+        device_id=(partner, tp),
+        device_id_type=MESH,
+    )
+    docs_copy.start()
 
     line = lax.broadcasted_iota(jnp.int32, (LANES, LANES), 0)
     lane = lax.broadcasted_iota(jnp.int32, (LANES, LANES), 1)
@@ -345,15 +399,15 @@
         row = docs_ext[0:1, b * LANES : (b + 1) * LANES].astype(F32)
         doc_cols[b * LANES : (b + 1) * LANES, :] = jnp.broadcast_to(row, (LANES, LANES)).T
 
-    low = lax.broadcasted_iota(jnp.int32, (2 * WIN, LANES), 1) < HD
+    left = lax.broadcasted_iota(jnp.int32, (2 * WIN, LANES), 1) < HD
     zero = jnp.zeros((2 * WIN, LANES), BF16)
 
     def attend_block(b, carry):
         start = pl.multiple_of(b * WIN, WIN)
         kv = kv_ext[pl.ds(start, 2 * WIN), 0:LANES]
         vk = kv_ext[pl.ds(start, 2 * WIN), LANES : 2 * LANES]
-        keys = jnp.concatenate([jnp.where(low, kv, zero), jnp.where(low, zero, vk)], axis=0)
-        values = jnp.concatenate([jnp.where(low, vk, zero), jnp.where(low, zero, kv)], axis=0)
+        keys = jnp.concatenate([jnp.where(left, kv, zero), jnp.where(left, zero, vk)], axis=0)
+        values = jnp.concatenate([jnp.where(left, vk, zero), jnp.where(left, zero, kv)], axis=0)
         query_doc = doc_cols[pl.ds(start + WIN, WIN), :]
         prev_doc = docs_ext[0:1, pl.ds(start, WIN)].astype(F32)
         this_doc = docs_ext[0:1, pl.ds(start + WIN, WIN)].astype(F32)
@@ -383,15 +437,18 @@
                 heads[...], proj[:, c * 512 : (c + 1) * 512], preferred_element_type=F32
             ).astype(BF16)
 
-        for k in range(2):
-            @pl.when(b == k + 1)
+        @pl.when(b == n_tp - 1)
+        def _():
+            plane_step(1)
+
+        for j in range(1, planes):
+            @pl.when(b == min(j, n_tp - 1))
             def _():
-                service(k)
+                service("col", 0, j)
 
         return carry
 
     lax.fori_loop(0, n_tp, attend_block, 0)
-    done = 2
 
     def rows_copy(peer, source):
         return pltpu.make_async_remote_copy(
@@ -405,63 +462,125 @@
 
     for peer in peers:
         rows_copy(peer, tp).start()
-    for k in range(done, 5):
-        service(k)
-    done = 5
     for peer in peers:
         rows_copy(peer, peer).wait_recv()
-    at = pl.multiple_of(PAD + tp * row_share, PAD)
     first = mix_scale * rest[...].astype(F32) + parts[tp].astype(F32)
     for peer in peers:
         first = first + parts_in[peer].astype(F32)
     mean = jnp.mean(first, axis=1, keepdims=True)
     first = first - mean
     var = jnp.mean(first * first, axis=1, keepdims=True)
-    normed[pl.ds(at, row_share), :] = (first * lax.rsqrt(var + norm_eps) * mix_ref[...]).astype(
-        BF16
-    )
-
-    service(done)
-    done += 1
-
-    def norm_copy(peer, source):
-        place = pl.ds(pl.multiple_of(PAD + source * row_share, PAD), row_share)
+    norm_own[...] = (first * lax.rsqrt(var + norm_eps) * mix_ref[...]).astype(BF16)
+
+    def workers(block):
+        parity = lax.rem(block // 2, 2)
+        return [
+            (block - 2 * parity + 2 * a, 2 * b + parity)
+            for a in (0, 1)
+            for b in range(n_tp // 2)
+        ]
+
+    def place_of(source):
+        return pl.ds(pl.multiple_of(PAD + source * row_share, PAD), row_share)
+
+    def norm_copy(i, device, source):
         return pltpu.make_async_remote_copy(
-            src_ref=normed.at[place],
-            dst_ref=normed.at[place],
-            send_sem=norm_send.at[peer],
+            src_ref=norm_own,
+            dst_ref=normed.at[place_of(source)],
+            send_sem=norm_send.at[i],
             recv_sem=norm_recv.at[source],
+            device_id=device,
+            device_id_type=MESH,
+        )
+
+    def is_me(device):
+        return (device[0] == sp) & (device[1] == tp)
+
+    def cols_copy(i, peer, source):
+        rows_at = pl.ds(pl.multiple_of(source * row_share, row_share), row_share)
+        return pltpu.make_async_remote_copy(
+            src_ref=norm_own.at[:, pl.ds(pl.multiple_of(peer * share, share), share)],
+            dst_ref=norm_cols.at[rows_at],
+            send_sem=cols_send.at[i],
+            recv_sem=cols_recv.at[source],
             device_id=(sp, peer),
             device_id_type=MESH,
         )
 
-    for peer in peers:
-        norm_copy(peer, tp).start()
-    for k in range(done, 9):
-        service(k)
-    done = 9
-    for peer in peers:
-        norm_copy(peer, peer).wait_recv()
-    tail = pltpu.make_async_remote_copy(
-        src_ref=normed.at[pl.ds(rows, PAD)],
-        dst_ref=normed.at[pl.ds(0, PAD)],
-        send_sem=halo_send.at[2],
-        recv_sem=halo_recv.at[2],
-        device_id=(after, tp),
-        device_id_type=MESH,
-    )
-    tail.start()
-    for k in range(done, early):
-        service(k)
-    tail.wait_recv()
-
-    place = lax.broadcasted_iota(jnp.int32, (rows, LANES), 0) + sp * rows
+    def tail_copy(i, device):
+        return pltpu.make_async_remote_copy(
+            src_ref=norm_own.at[pl.ds(row_share - PAD, PAD)],
+            dst_ref=normed.at[pl.ds(0, PAD)],
+            send_sem=tail_send.at[i],
+            recv_sem=tail_recv,
+            device_id=device,
+            device_id_type=MESH,
+        )
+
+    own_workers = workers(sp)
+    next_workers = workers(after)
+    for i, device in enumerate(own_workers):
+        @pl.when(jnp.logical_not(is_me(device)))
+        def _():
+            norm_copy(i, device, tp).start()
+
+    @pl.when(tp == n_tp - 1)
+    def _():
+        for i, device in enumerate(next_workers):
+            tail_copy(i, device).start()
+
+    for i, peer in enumerate(peers):
+        cols_copy(i, peer, tp).start()
+    service("col", 1, 1)
+    plane_step(2)
+
+    @pl.when(home)
+    def _():
+        normed[place_of(tp), :] = norm_own[...]
+
+    norm_cols[pl.ds(pl.multiple_of(tp * row_share, row_share), row_share), :] = norm_own[
+        :, pl.ds(pl.multiple_of(tp * share, share), share)
+    ]
+    for j in range(planes):
+        service("row", 0, j)
+    for j in range(2, planes):
+        service("col", 1, j)
+    service("own", 2, 0)
+    for j in range(planes):
+        service("row", 1, j)
+    docs_copy.wait_recv()
+    for b in range(rows // LANES + 1):
+        part = slice(b * LANES, (b + 1) * LANES)
+        row = jnp.where(home, docs_ext[0:1, part], docs_other[0:1, part]).astype(F32)
+        work_cols[part, :] = jnp.broadcast_to(row, (LANES, LANES)).T
+
+    for source in range(n_tp):
+        @pl.when(jnp.logical_not(home & (tp == source)))
+        def _():
+            norm_copy(0, (sp, sibling), source).wait_recv()
+
+    tail_copy(0, (sp, sibling)).wait_recv()
+
+    @pl.when(home)
+    def _():
+        for copy in settle:
+            copy.wait()
+
+    @pl.when(jnp.logical_not(home))
+    def _():
+        for copy in taps:
+            copy.wait_recv()
+        for w in (0, 1):
+            for index in range(n):
+                await_block(w, index)
+
+    place = lax.broadcasted_iota(jnp.int32, (rows, LANES), 0) + work * rows
 
     def convolved(source, taps_ref, at):
         total = taps_ref[0:1, pl.ds(at, LANES)] * source[PAD : PAD + rows, :]
-        doc = doc_cols[WIN : WIN + rows, :]
+        doc = work_cols[WIN : WIN + rows, :]
         for lag in range(1, TAPS):
-            same = (doc_cols[WIN - lag : WIN - lag + rows, :] == doc) & (place >= lag)
+            same = (work_cols[WIN - lag : WIN - lag + rows, :] == doc) & (place >= lag)
             shifted = jnp.where(same, source[PAD - lag : PAD - lag + rows, :], 0.0)
             total = total + taps_ref[lag : lag + 1, pl.ds(at, LANES)] * shifted
         return total
@@ -475,18 +594,30 @@
         both = both.astype(BF16).astype(F32)
         up_gate[...] = both[:, :LANES]
         up_value[...] = both[:, LANES:]
-        gate = convolved(up_gate, gate_taps_ref, at)
-        value = convolved(up_value, value_taps_ref, at)
+        gate = convolved(up_gate, taps_gate, at)
+        value = convolved(up_value, taps_value, at)
         inner = math.sqrt(2.0 / math.pi) * (gate + 0.044715 * (gate * gate * gate))
         hidden[:, pl.ds(at, LANES)] = (0.5 * gate * (1.0 + jnp.tanh(inner)) * value).astype(BF16)
-        for k, when in ((0, 3), (1, 6), (2, 9)):
-            @pl.when(c == when)
+        for j in range(1, planes):
+            @pl.when(c == 3 * j - 2)
             def _():
-                service(early + k)
+                service("col", 2, j)
+
+        for j in (0, 1):
+            @pl.when(c == 6 + 2 * j)
+            def _():
+                service("row", 2, j)
 
         return carry
 
     lax.fori_loop(0, ff // LANES, up_block, 0)
+    for j in range(2, planes):
+        service("row", 2, j)
+
+    @pl.when(jnp.logical_not(home))
+    def _():
+        for index in range(n):
+            await_block(2, index)
 
     def term_copy(index, source):
         owner = index // per
@@ -495,48 +626,52 @@
             dst_ref=terms_in.at[source, lax.rem(index, per)],
             send_sem=term_send.at[index],
             recv_sem=term_recv.at[source, lax.rem(index, per)],
-            device_id=(sp, owner),
+            device_id=(work, owner),
             device_id_type=MESH,
         )
 
     def down_block(q, carry):
-        for k in range(3, len(last)):
-            @pl.when(q == 2 * (last[k][1] - 1) + 1)
-            def _():
-                service(early + k)
-
-        distance = (q + 1) // 2
-        index = ring_index(jnp.where(lax.rem(q, 2) == 1, here - distance, here + distance), n)
+        index = lax.rem(q + per * 2 * (1 - x), n)
         terms[index] = jnp.dot(
             hidden[...], down_all[index], preferred_element_type=F32
         ).astype(BF16)
 
-        @pl.when(index // per != tp)
+        mine = home & (index // per == tp)
+
+        @pl.when(mine)
         def _():
-            term_copy(index, tp).start()
+            terms_in[tp, lax.rem(index, per)] = terms[index]
+
+        @pl.when(jnp.logical_not(mine))
+        def _():
+            term_copy(index, unit).start()
 
         return carry
 
     lax.fori_loop(0, n, down_block, 0)
 
-    for peer in peers:
-        for j in range(per):
-            pltpu.make_async_remote_copy(
-                src_ref=terms_in.at[peer, j],
-                dst_ref=terms_in.at[peer, j],
-                send_sem=term_send.at[0],
-                recv_sem=term_recv.at[peer, j],
-                device_id=(sp, peer),
-                device_id_type=MESH,
-            ).wait_recv()
+    for source in range(n_tp):
+        @pl.when(jnp.logical_not(home & (tp == source)))
+        def _():
+            for j in range(per):
+                pltpu.make_async_remote_copy(
+                    src_ref=terms_in.at[source, j],
+                    dst_ref=terms_in.at[source, j],
+                    send_sem=term_send.at[0],
+                    recv_sem=term_recv.at[source, j],
+                    device_id=(sp, sibling),
+                    device_id_type=MESH,
+                ).wait_recv()
+
+    for i, peer in enumerate(peers):
+        cols_copy(i, peer, peer).wait_recv()
 
     sums = jnp.zeros((rows, 1), F32)
     squares = jnp.zeros((rows, 1), F32)
     for j in range(per):
-        mine = normed[PAD:, pl.ds(pl.multiple_of(tp * share + j * cols, cols), cols)]
-        total = mix_scale * mine.astype(F32) + terms[tp * per + j].astype(F32)
-        for peer in peers:
-            total = total + terms_in[peer, j].astype(F32)
+        total = mix_scale * norm_cols[:, j * cols : (j + 1) * cols].astype(F32)
+        for source in range(n_tp):
+            total = total + terms_in[source, j].astype(F32)
         second[:, j * cols : (j + 1) * cols] = total
         sums = sums + jnp.sum(total, axis=1, keepdims=True)
         squares = squares + jnp.sum(total * total, axis=1, keepdims=True)
@@ -568,21 +703,39 @@
         (second[...] - mean) * lax.rsqrt(var + norm_eps) * final_ref[...]
     ).astype(BF16)
 
-    for w in range(3):
-        for way in (0, 1):
-            for step in range(1, steps + 1):
-                for half in (0, 1):
-                    if step < steps or half == way:
-                        sending(w, way, step, half).wait_send()
+    plane_step(3)
+
+    @pl.when(home)
+    def _():
+        for w in range(3):
+            for at in range(planes):
+                to_row(w, at, slot(w, sp)).wait_send()
+            for index in range(n):
+                to_core(w, index, slot(w, index)).wait_send()
+        for copy in taps:
+            copy.wait_send()
+
     for copy in halo:
         copy.wait_send()
-    tail.wait_send()
-    for peer in peers:
+    docs_copy.wait_send()
+    for i, device in enumerate(own_workers):
+        @pl.when(jnp.logical_not(is_me(device)))
+        def _():
+            norm_copy(i, device, tp).wait_send()
+
+    @pl.when(tp == n_tp - 1)
+    def _():
+        for i, device in enumerate(next_workers):
+            tail_copy(i, device).wait_send()
+
+    for i, peer in enumerate(peers):
         rows_copy(peer, tp).wait_send()
-        norm_copy(peer, tp).wait_send()
+        cols_copy(i, peer, tp).wait_send()
         stat_copy(peer, tp).wait_send()
-        for j in range(per):
-            term_copy(peer * per + j, tp).wait_send()
+    for index in range(n):
+        @pl.when(jnp.logical_not(home & (tp == index // per)))
+        def _():
+            term_copy(index, unit).wait_send()
 
 
 def fused(
@@ -608,7 +761,7 @@
     depth, ff = gate_proj.shape
     cols = down_proj.shape[1]
     per = width // n_tp // cols
-    steps = n // 2
+    planes = n // 2
     kv = jnp.concatenate([key_rows, value_rows, value_rows, key_rows], axis=1)
     docs = jnp.broadcast_to(doc_ids[None, :], (8, rows))
     share = rows // n_tp
@@ -621,7 +774,7 @@
         out_shape=jax.ShapeDtypeStruct((rows, width // n_tp), BF16),
         in_specs=[
             anywhere, anywhere, smem, anywhere, anywhere, anywhere, vmem,
-            anywhere, anywhere, vmem, vmem, anywhere, vmem,
+            anywhere, anywhere, anywhere, anywhere, anywhere, vmem,
         ],
         out_specs=vmem,
         scratch_shapes=[
@@ -630,13 +783,19 @@
             pltpu.VMEM((n, ff, cols), BF16),
             pltpu.VMEM((WIN + rows, 4 * HD), BF16),
             pltpu.VMEM((8, WIN + rows), jnp.int32),
+            pltpu.VMEM((8, WIN + rows), jnp.int32),
             pltpu.VMEM((WIN + rows, LANES), F32),
+            pltpu.VMEM((WIN + rows, LANES), F32),
+            pltpu.VMEM(gate_taps.shape, F32),
+            pltpu.VMEM(gate_taps.shape, F32),
             pltpu.VMEM((rows, head_cols), BF16),
             pltpu.VMEM((head_cols, width), BF16),
             pltpu.VMEM((share, width), BF16),
             pltpu.VMEM((share, head_cols), BF16),
             pltpu.VMEM((n_tp, share, width), BF16),
             pltpu.VMEM((n_tp, share, width), BF16),
+            pltpu.VMEM((share, width), BF16),
+            pltpu.VMEM((rows, width // n_tp), BF16),
             pltpu.VMEM((PAD + rows, width), BF16),
             pltpu.VMEM((PAD + rows, LANES), F32),
             pltpu.VMEM((PAD + rows, LANES), F32),
@@ -645,15 +804,23 @@
             pltpu.VMEM((n_tp, per, rows, cols), BF16),
             pltpu.VMEM((rows, width // n_tp), F32),
             pltpu.VMEM((n_tp, 8, rows), F32),
-            dma((3, 2, steps, 2)),
-            dma((3, 2, steps, 2)),
-            dma((8,)),
+            dma((3, planes // 2)),
+            dma((3, planes)),
+            dma((3, n)),
+            dma((3, n)),
+            dma((10,)),
+            dma((2,)),
+            dma((2,)),
             dma((3,)),
             dma((3,)),
             dma((n_tp,)),
             dma((n_tp,)),
             dma((n_tp,)),
             dma((n_tp,)),
+            dma((n_tp,)),
+            dma((n_tp,)),
+            dma((n_tp,)),
+            dma(()),
             dma((n,)),
             dma((n_tp, per)),
             dma((n_tp,)),
@@ -687,8 +854,10 @@
     depth, ff = gate_proj.shape
     cols = down_proj.shape[1]
     fits = (
-        n % 2 == 0
+        n % 4 == 0
+        and n_tp == 4
         and n >= 8
+        and n <= n_tp * 2
         and ff >= 10 * LANES
         and query_rows.shape[0] == n_tp * WIN
         and key_rows.shape[1] == HD

time: 201 us -> 180 us (0.90)
  Pallas kernels: 194 us -> 171 us
    pallas_call x1, Pallas kernels: 194 us -> 171 us  [fused(): pl.pallas_call(functools.partial(layer_kernel, n, n_tp), out_shape=jax.Sh...]
where the time goes in v2:
time: 180 us; the launch traced here: 177 us
  Pallas kernels  171 us (95%)
  local copies, waits for them, and re-layouts  5.06 us (3%)
    pallas_call x1, Pallas kernels, fused(): pl.pallas_call(functools.partial(layer_kernel, n, n_tp), out_shape=jax.Sh...  171 us
    unnamed x3, local copies, waits for them, and re-layouts  3.78 us

profile of v2, /device:TPU:0, one launch (start us, length us, event | category | flops | bytes accessed | tf_op | source)
XLA Modules:
  0.0 177.0 jit_solution(13203863922392797569)
XLA Ops:
  0.0 1.3 broadcast_in_dim.12.docs_ref
  1.3 1.0 copy.15
  2.2 1.0 copy.16
  3.2 0.9 pad_maximum_fusion.kv_ref
  4.1 171.0 %layer.1 = bf16[512,512]{1,0:T(8,128)(2,1)} custom-call(bf16[512,256]{1,0:T(8,128)(2,1)} %pad_maximum_fusion.kv_ref, s32[8,512]{1,0:T(8,128)} %broadcast_in_dim.12.docs_ref, f32[8]{0:T(128)} %sink_ref.1, bf16[512,512]{1,0:T(8,128)(2,1)} %query_ref.1, bf16[512,2048]{1,0:T(8,128)(2,1)} %out_proj_ref.1, bf16[512,2048]{1,0:T(8,128)(2,1)} %residual_ref.1, ...), custom_call_target="tpu_custom_call" | custom-call | tf_op jit(solution)/shard_map/layer/pallas_call | solution.py:772
  175.1 1.9 %copy.20 = bf16[512,512]{1,0:T(8,128)(2,1)} copy(bf16[512,512]{1,0:T(8,128)(2,1)} %layer.1) | data formatting | bytes 1048576
